TPU v7x, 32 devices: a whole 2x2x4 slice. The times are simulated.
32 devices in a mesh: grp: 2 (over y), fs: 4 (over z), tp: 4 (over x, core).
Axes of the slice: x: 2, y: 2, z: 4, core: 2. Of those that a mesh axis runs over, the one named last changes fastest.
Arguments:
- tokens: bfloat16 [3072, 2048], P(('grp', 'fs')), parts along dimension 0, may hold values from -3 to 3
- gate_weight: bfloat16 [2048, 5120], P('fs', 'tp'), may hold values from -0.125 to 0.125
- up_weight: bfloat16 [2048, 5120], P('fs', 'tp'), may hold values from -0.125 to 0.125
- down_weight: bfloat16 [5120, 2048], P('tp', 'fs'), may hold values from -0.078125 to 0.078125
- pool_weight: bfloat16 [512, 4, 512], P('fs', None, 'tp'), may hold values from -0.375 to 0.375
- pool_bias: float32 [4, 512], replicated, may hold values from -3 to 3
- pool_scale: float32 [2048], replicated, may hold values from 0.1 to 1.9
- gain_first: float32 [2048], replicated, may hold values from 0.1 to 1.9
- gain_mix: float32 [2048], replicated, may hold values from 0.1 to 1.9
- gain_second: float32 [2048], replicated, may hold values from 0.1 to 1.9
Outputs:
- result: bfloat16 [3072, 2048], P(('grp', 'fs')), parts along dimension 0
There are 2 independent parts, one for each index of `grp`. A program takes and returns all parts, laid end to end along the dimension named above; an argument that names none is the same for every part. Nothing has to cross between parts.
All inputs are finite; a program needn't handle non-finite values.
Results may differ from a plain program's by a relative error of at most 0.018.
Values may be sent and summed in bfloat16 or wider, within the bound.
A program may use at most 64 MiB of HBM per device.

v0:
```python
import jax
import jax.numpy as jnp
from jax import lax
from jax.sharding import PartitionSpec as P

eps = 1e-06
pool_spans = (2, 4, 8, 16)
pad_width = 8


def rms_scale(values, gain_vec):
    fvalues = values.astype(jnp.float32)
    scaled = fvalues * lax.rsqrt(jnp.mean(fvalues * fvalues, axis=-1, keepdims=True) + eps)
    return (scaled * gain_vec).astype(jnp.bfloat16)


def ffn_hidden(normed, gate_full, up_full):
    gate_proj = jnp.dot(normed, gate_full, preferred_element_type=jnp.float32)
    up_proj = jnp.dot(normed, up_full, preferred_element_type=jnp.float32)
    return (jax.nn.silu(gate_proj) * up_proj).astype(jnp.bfloat16)


def pool_block(padded, offset, seq_len, pool_full, pool_bias, pool_scale):
    n_tokens = padded.shape[0] - 2 * pad_width
    group_width = pool_full.shape[0]
    position = offset + lax.iota(jnp.int32, n_tokens)
    column_pos = offset - pad_width + lax.iota(jnp.int32, padded.shape[0])
    center = padded[pad_width : pad_width + n_tokens].astype(jnp.float32)
    outputs = []
    for group_number, window_span in enumerate(pool_spans):
        low_edge = jnp.clip(position - window_span // 2, 0, seq_len)
        high_edge = jnp.clip(position - window_span // 2 + window_span, 0, seq_len)
        band_mask = (
            (column_pos[None, :] >= low_edge[:, None]) & (column_pos[None, :] < high_edge[:, None])
        ).astype(jnp.bfloat16)
        lower_col = group_number * group_width
        columns = padded[:, lower_col : lower_col + group_width]
        window_sum = jnp.dot(band_mask, columns, preferred_element_type=jnp.float32)
        window_mean = window_sum / (high_edge - low_edge).astype(jnp.float32)[:, None]
        deviation = (window_mean - center[:, lower_col : lower_col + group_width]).astype(
            jnp.bfloat16
        )
        mapped = jnp.dot(
            deviation, pool_full[:, group_number, :], preferred_element_type=jnp.float32
        )
        outputs.append(mapped + pool_bias[group_number])
    return jnp.concatenate(outputs, axis=-1) * pool_scale


def shards(
    tokens,
    gate_weight,
    up_weight,
    down_weight,
    pool_weight,
    pool_bias,
    pool_scale,
    gain_first,
    gain_mix,
    gain_second,
):
    gate_full, up_full, pool_half = (
        lax.all_gather(gate_weight, "fs", axis=0, tiled=True),
        lax.all_gather(up_weight, "fs", axis=0, tiled=True),
        lax.all_gather(pool_weight, "fs", axis=0, tiled=True),
    )
    down_full = lax.all_gather(down_weight, "fs", axis=1, tiled=True)
    pool_full = lax.all_gather(pool_half, "tp", axis=2, tiled=True)
    seq_len = tokens.shape[0]
    first_normed = rms_scale(tokens, gain_first)
    first_hidden = ffn_hidden(first_normed, gate_full, up_full)
    second_gate, second_up, second_down = (gate_full, up_full, down_full)
    first_branch = lax.psum(
        jnp.dot(first_hidden, down_full, preferred_element_type=jnp.float32).astype(jnp.bfloat16),
        "tp",
    ).astype(jnp.float32)
    after_first = (tokens.astype(jnp.float32) + 0.5 * first_branch).astype(jnp.bfloat16)
    mix_normed = rms_scale(after_first, gain_mix)
    padded = jnp.pad(mix_normed, ((pad_width, pad_width), (0, 0)))
    mixed = pool_block(padded, 0, seq_len, pool_full, pool_bias, pool_scale)
    after_mix = (after_first.astype(jnp.float32) + mixed).astype(jnp.bfloat16)
    second_normed = rms_scale(after_mix, gain_second)
    second_hidden = ffn_hidden(second_normed, second_gate, second_up)
    second_branch = lax.psum(
        jnp.dot(second_hidden, second_down, preferred_element_type=jnp.float32).astype(
            jnp.bfloat16
        ),
        "tp",
    ).astype(jnp.float32)
    return (after_mix.astype(jnp.float32) + 0.5 * second_branch).astype(jnp.bfloat16)


def solution(mesh):
    return jax.shard_map(
        shards,
        mesh=mesh,
        in_specs=(
            P(("grp", "fs"), None),
            P("fs", "tp"),
            P("fs", "tp"),
            P("tp", "fs"),
            P("fs", None, "tp"),
            P(),
            P(),
            P(),
            P(),
            P(),
        ),
        out_specs=P(("grp", "fs"), None),
        check_vma=False,
    )
```

profile of v0, /device:TPU:0, one launch (start us, length us, event | category | flops | bytes accessed | tf_op | source)
XLA Modules:
  0.0 468.3 jit_solution(4957366809883981244)
XLA Ops:
  6.5 0.0 copy-start
  6.5 0.0 copy-start.8
  6.5 0.0 all-gather.5.cloned.1.call-start
  6.5 0.7 all-gather.5.cloned.1.call-update
  7.3 0.0 all-gather.7.cloned.1.call-start
  7.3 0.7 all-gather.7.cloned.1.call-update
  8.0 0.0 all-gather.9.cloned.1.call-start
  8.1 0.7 all-gather.9.cloned.1.call-update
  8.7 0.0 all-reduce.4.cloned.1.call-start
  8.8 0.0 copy-done
  8.8 0.4 fusion
  9.2 100.5 %all-gather.5.cloned.1.call-done = bf16[2048,1280]{1,0:T(8,128)(2,1)} async-done(((bf16[512,1280]{1,0:T(8,128)(2,1)}), bf16[2048,1280]{1,0:T(8,128)(2,1)}) %all-gather.5.cloned.1.call-update) | async-done | bytes 5242896 | tf_op jit(solution)/shard_map/all_gather | solution.py:63
  109.7 0.0 copy-done.8
  109.7 6.0 %fusion.56 = f32[384,1280]{1,0:T(8,128)} fusion(bf16[2048,1280]{1,0:T(8,128)(2,1)} %all-gather.5.cloned.1.call-done, bf16[384,2048]{1,0:T(8,128)(2,1)S(1)} %copy-done, f32[2048]{0:T(1024)S(1)} %copy-done.8, f32[384]{0:T(512)S(1)} %add_rsqrt_fusion.2), kind=kOutput, calls=%fused_computation.69 | convolution fusion | flops 2016411648 | bytes 8791552 | tf_op jit(solution)/shard_map/dot_general | solution.py:18
  115.7 0.0 copy-start.4
  115.7 0.0 copy-start.7
  115.7 92.0 %all-gather.7.cloned.1.call-done = bf16[2048,1280]{1,0:T(8,128)(2,1)} async-done(((bf16[512,1280]{1,0:T(8,128)(2,1)}), bf16[2048,1280]{1,0:T(8,128)(2,1)}) %all-gather.7.cloned.1.call-update) | async-done | bytes 5242896 | tf_op jit(solution)/shard_map/all_gather | solution.py:64
  207.7 98.0 %all-gather.9.cloned.1.call-done = bf16[1280,2048]{1,0:T(8,128)(2,1)} async-done(((bf16[1280,512]{1,0:T(8,128)(2,1)}), bf16[1280,2048]{1,0:T(8,128)(2,1)}) %all-gather.9.cloned.1.call-update) | async-done | bytes 5242896 | tf_op jit(solution)/shard_map/all_gather | solution.py:67
  305.6 10.6 %convolution_convert_fusion.1 = bf16[384,2048]{1,0:T(8,128)(2,1)} fusion(bf16[1280,2048]{1,0:T(8,128)(2,1)} %all-gather.9.cloned.1.call-done, bf16[2048,1280]{1,0:T(8,128)(2,1)} %all-gather.7.cloned.1.call-done, f32[384,1280]{1,0:T(8,128)} %fusion.56, bf16[384,2048]{1,0:T(8,128)(2,1)S(1)} %copy-done, f32[2048]{0:T(1024)S(1)} %copy-done.8, ...), kind=kOutput, calls=%fused_computation.25 | convolution fusion | flops 4033413120 | bytes 15607296 | tf_op jit(solution)/shard_map/dot_general | solution.py:74
  316.3 0.0 copy-start.5
  316.3 0.0 all-reduce.4.cloned.1.call-update
  316.3 0.0 all-gather.11.cloned.1.call-start
  316.4 0.0 copy-done.4
  316.4 16.7 %all_gather.18 = bf16[512,4,128]{2,0,1:T(8,128)(2,1)} all-gather(bf16[128,4,128]{2,0,1:T(8,128)(2,1)S(1)} %copy.11), channel_id=1, replica_groups=mesh['grp'=2,'fs'=4,'tp'=4] {'fs'}, dimensions={0}, use_global_device_ids=true | all-gather | bytes 655360 | tf_op jit(solution)/shard_map/all_gather | solution.py:65
  333.1 0.0 all-gather.11.cloned.1.call-update
  333.1 0.2 all-reduce.6.cloned.1.call-start
  333.4 0.0 copy-done.7
  333.4 24.2 %all-reduce.4.cloned.1.call-done = bf16[384,2048]{1,0:T(8,128)(2,1)} async-done(((bf16[384,2048]{1,0:T(8,128)(2,1)}), bf16[384,2048]{1,0:T(8,128)(2,1)}) %all-reduce.4.cloned.1.call-update) | async-done | bytes 1572880 | tf_op jit(solution)/shard_map/psum | solution.py:73
  357.7 2.2 fusion.4
  359.9 0.0 copy-done.5
  359.9 0.0 copy-done.1
  359.9 3.0 fusion.97
  362.9 19.0 %all-gather.11.cloned.1.call-done = bf16[512,4,512]{2,0,1:T(8,128)(2,1)} async-done(((bf16[512,4,128]{2,0,1:T(8,128)(2,1)}), bf16[512,4,512]{2,0,1:T(8,128)(2,1)}) %all-gather.11.cloned.1.call-update) | async-done | bytes 2097168 | tf_op jit(solution)/shard_map/all_gather | solution.py:68
  382.0 3.0 convolution_add_fusion
  384.9 3.0 convolution_add_fusion.1
  387.9 3.0 convolution_add_fusion.2
  390.9 3.0 convolution_add_fusion.3
  393.9 0.0 copy-done.6
  393.9 2.9 fusion.8
  396.8 0.0 copy-start.2
  396.8 1.1 copy-done.2
  398.0 0.0 copy-done.9
  398.0 6.0 %fusion.52 = f32[384,1280]{1,0:T(8,128)} fusion(bf16[2048,1280]{1,0:T(8,128)(2,1)} %all-gather.5.cloned.1.call-done, bf16[384,2048]{1,0:T(8,128)(2,1)S(1)} %get-tuple-element.6, f32[2048]{0:T(1024)S(1)} %copy-done.9, f32[384]{0:T(512)S(1)} %add_rsqrt_fusion), kind=kOutput, calls=%fused_computation.68 | convolution fusion | flops 2016411648 | bytes 8791552 | tf_op jit(solution)/shard_map/dot_general | solution.py:18
  404.0 11.2 %convolution_convert_fusion = bf16[384,2048]{1,0:T(8,128)(2,1)} fusion(bf16[1280,2048]{1,0:T(8,128)(2,1)} %all-gather.9.cloned.1.call-done, bf16[2048,1280]{1,0:T(8,128)(2,1)} %all-gather.7.cloned.1.call-done, f32[384,1280]{1,0:T(8,128)} %fusion.52, bf16[384,2048]{1,0:T(8,128)(2,1)} %copy-done.2, f32[2048]{0:T(1024)S(1)} %copy-done.9, f32[384]{0:T(512)S(1)} %add_rsqrt_fusion), kind=kOutput, calls=%fused_computation.24 | convolution fusion | flops 4033413120 | bytes 15607296 | tf_op jit(solution)/shard_map/dot_general | solution.py:85
  415.2 0.0 all-reduce.6.cloned.1.call-update
  415.2 43.0 %all-reduce.6.cloned.1.call-done = bf16[384,2048]{1,0:T(8,128)(2,1)} async-done(((bf16[384,2048]{1,0:T(8,128)(2,1)}), bf16[384,2048]{1,0:T(8,128)(2,1)}) %all-reduce.6.cloned.1.call-update) | async-done | bytes 1572880 | tf_op jit(solution)/shard_map/psum | solution.py:84
  458.2 0.0 copy-done.3
  458.2 3.2 fusion.11
  (18 shorter events, 0.1 us)
Async XLA Ops:
  6.5 2.3 copy-start
  6.5 103.2 %copy-start.8 = (f32[2048]{0:T(1024)S(1)}, f32[2048]{0:T(1024)}, u32[]{:S(2)}) copy-start(f32[2048]{0:T(1024)} %param.17) | copy-start | bytes 24580
  6.5 103.2 %all-gather.5.cloned.1.call-start = ((), (), s32[]{:S(2)}) async-start(), calls=%async_computation | async-start | bytes 6553600 | tf_op jit(solution)/shard_map/all_gather | solution.py:63
  7.3 200.4 %all-gather.7.cloned.1.call-start = ((), (), s32[]{:S(2)}) async-start(), calls=%async_computation.1 | async-start | bytes 6553600 | tf_op jit(solution)/shard_map/all_gather | solution.py:64
  8.0 297.6 %all-gather.9.cloned.1.call-start = ((), (), s32[]{:S(2)}) async-start(), calls=%async_computation.2 | async-start | bytes 6553600 | tf_op jit(solution)/shard_map/all_gather | solution.py:67
  8.7 348.9 %all-reduce.4.cloned.1.call-start = ((), (), s32[]{:S(2)}) async-start(), calls=%async_computation.3 | async-start | bytes 3145728 | tf_op jit(solution)/shard_map/psum | solution.py:73
  115.7 200.7 %copy-start.4 = (bf16[128,4,128]{2,1,0:T(4,128)(2,1)S(1)}, bf16[128,4,128]{2,1,0:T(4,128)(2,1)}, u32[]{:S(2)}) copy-start(bf16[128,4,128]{2,1,0:T(4,128)(2,1)} %param.14) | copy-start | bytes 393220
  115.7 217.7 %copy-start.7 = (f32[4,512]{1,0:T(4,128)S(1)}, f32[4,512]{1,0:T(4,128)}, u32[]{:S(2)}) copy-start(f32[4,512]{1,0:T(4,128)} %param.15) | copy-start | bytes 24580
  316.3 43.6 %copy-start.5 = (f32[2048]{0:T(1024)S(1)}, f32[2048]{0:T(1024)}, u32[]{:S(2)}) copy-start(f32[2048]{0:T(1024)} %param.18) | copy-start | bytes 24580
  316.3 65.6 %all-gather.11.cloned.1.call-start = ((), (), s32[]{:S(2)}) async-start(), calls=%async_computation.4 | async-start | bytes 2621440 | tf_op jit(solution)/shard_map/all_gather | solution.py:68
  333.1 125.1 %all-reduce.6.cloned.1.call-start = ((), (), s32[]{:S(2)}) async-start(), calls=%async_computation.5 | async-start | bytes 3145728 | tf_op jit(solution)/shard_map/psum | solution.py:84
  357.6 2.2 copy-start.1
  390.9 3.0 copy-start.6
  393.9 4.1 copy-start.9
  396.8 1.1 copy-start.2
  404.0 54.2 %copy-start.3 = (bf16[384,2048]{1,0:T(8,128)(2,1)S(1)}, bf16[384,2048]{1,0:T(8,128)(2,1)}, u32[]{:S(2)}) copy-start(bf16[384,2048]{1,0:T(8,128)(2,1)} %copy-done.2) | copy-start | bytes 4718596
Sparse Core Ops, SparseCore 0:
  8.9 100.7 all-gather.4
  111.3 96.3 all-gather.6
  209.2 96.3 all-gather.8
  316.4 41.1 all-reduce.3
  359.0 22.8 all-gather.10
  415.3 42.8 all-reduce.5
where the time goes:
time: 469 us; the launch traced here: 468 us
  waiting for transfers between devices  379 us (81%)
  matrix products  45.8 us (10%)
  blocking collectives  16.7 us (4%)
  between operations  13.6 us (3%)
  other arithmetic  11.8 us (3%)
    all_gather x1, waiting for transfers between devices, shards(): lax.all_gather(gate_weight, 'fs', axis=0, tiled=True)  101 us
    all_gather x1, waiting for transfers between devices, shards(): down_full = lax.all_gather(down_weight, 'fs', axis=1, tiled=True)  98 us
    all_gather x1, waiting for transfers between devices, shards(): lax.all_gather(up_weight, 'fs', axis=0, tiled=True)  92 us
    psum x1, waiting for transfers between devices, shards(): lax.psum(jnp.dot(second_hidden, second_down, preferred_element_type=jnp.f...  43 us
    psum x1, waiting for transfers between devices, shards(): lax.psum(jnp.dot(first_hidden, down_full, preferred_element_type=jnp.floa...  24.2 us
    all_gather x1, waiting for transfers between devices, shards(): pool_full = lax.all_gather(pool_half, 'tp', axis=2, tiled=True)  19 us
    all_gather x1, blocking collectives, shards(): lax.all_gather(pool_weight, 'fs', axis=0, tiled=True)  16.7 us
    dot_general x2, matrix products, ffn_hidden(): gate_proj = jnp.dot(normed, gate_full, preferred_element_type=jnp.float32)  12 us
  transfers between devices with their start and end apart: 6, of which 6 were waited for; matrix products, arithmetic and copies ran while one was open for 3% of the time, Pallas kernels for 0%

commit v1 on v0

--- a/solution.py
+++ b/solution.py
@@ -64,7 +64,12 @@
         lax.all_gather(up_weight, "fs", axis=0, tiled=True),
         lax.all_gather(pool_weight, "fs", axis=0, tiled=True),
     )
-    down_full = lax.all_gather(down_weight, "fs", axis=1, tiled=True)
+    ring = [down_weight]
+    for hop in range(3):
+        ring.append(lax.ppermute(ring[-1], "fs", [(dev, (dev + 1) % 4) for dev in range(4)]))
+    down_full = jnp.roll(
+        jnp.concatenate(ring[::-1], axis=1), (lax.axis_index("fs") + 1) * ring[0].shape[1], axis=1
+    )
     pool_full = lax.all_gather(pool_half, "tp", axis=2, tiled=True)
     seq_len = tokens.shape[0]
     first_normed = rms_scale(tokens, gain_first)

time: 469 us -> 433 us (0.923)
  waiting for transfers between devices: 379 us -> 289 us
  starting transfers between devices: 0.38 us -> 39 us
  local copies, waits for them, and re-layouts: 1.19 us -> 16.6 us
    ppermute x0 -> x3, waiting for transfers between devices: none -> 156 us  [shards(): lax.ppermute(ring[-1], 'fs', [(dev, (dev + 1) % 4) for dev in range(4)])]
    all_gather x1, waiting for transfers between devices: 101 us -> 0.01 us  [shards(): lax.all_gather(gate_weight, 'fs', axis=0, tiled=True)]
    all_gather x1 -> x0, waiting for transfers between devices: 98 us -> none  [shards(): down_full = lax.all_gather(down_weight, 'fs', axis=1, tiled=True)]
    all_gather x1, waiting for transfers between devices: 92 us -> 45.3 us  [shards(): lax.all_gather(up_weight, 'fs', axis=0, tiled=True)]
    ppermute x0 -> x3, starting transfers between devices: none -> 38.7 us  [shards(): lax.ppermute(ring[-1], 'fs', [(dev, (dev + 1) % 4) for dev in range(4)])]
    unnamed x21 -> x30, local copies, waits for them, and re-layouts: 1.18 us -> 15.3 us
  transfers between devices with their start and end apart: 6 -> 8, of which waited for: 6 -> 7; matrix products, arithmetic and copies ran while one was open for 3% -> 6% of each run, Pallas kernels for 0% -> 0%
where the time goes in v1:
time: 433 us; the launch traced here: 432 us
  waiting for transfers between devices  289 us (67%)
  matrix products  45.8 us (11%)
  starting transfers between devices  39 us (9%)
  blocking collectives  16.7 us (4%)
  local copies, waits for them, and re-layouts  16.6 us (4%)
  between operations  13.3 us (3%)
  other arithmetic  11.8 us (3%)
    ppermute x3, waiting for transfers between devices, shards(): lax.ppermute(ring[-1], 'fs', [(dev, (dev + 1) % 4) for dev in range(4)])  156 us
    all_gather x1, waiting for transfers between devices, shards(): lax.all_gather(up_weight, 'fs', axis=0, tiled=True)  45.3 us
    psum x1, waiting for transfers between devices, shards(): lax.psum(jnp.dot(second_hidden, second_down, preferred_element_type=jnp.f...  43 us
    ppermute x3, starting transfers between devices, shards(): lax.ppermute(ring[-1], 'fs', [(dev, (dev + 1) % 4) for dev in range(4)])  38.7 us
    psum x1, waiting for transfers between devices, shards(): lax.psum(jnp.dot(first_hidden, down_full, preferred_element_type=jnp.floa...  24.9 us
    all_gather x1, waiting for transfers between devices, shards(): pool_full = lax.all_gather(pool_half, 'tp', axis=2, tiled=True)  19.1 us
    all_gather x1, blocking collectives, shards(): lax.all_gather(pool_weight, 'fs', axis=0, tiled=True)  16.7 us
    unnamed x30, local copies, waits for them, and re-layouts  15.3 us
  transfers between devices with their start and end apart: 8, of which 7 were waited for; matrix products, arithmetic and copies ran while one was open for 6% of the time, Pallas kernels for 0%

profile of v1, /device:TPU:0, one launch (start us, length us, event | category | flops | bytes accessed | tf_op | source)
XLA Modules:
  0.0 432.4 jit_solution(7002920872208513743)
XLA Ops:
  6.5 0.0 all-gather.4.cloned.1.call-start
  6.5 0.7 all-gather.4.cloned.1.call-update
  7.3 0.0 all-gather.6.cloned.1.call-start
  7.3 0.7 all-gather.6.cloned.1.call-update
  8.0 0.0 all-reduce.4.cloned.1.call-start
  8.1 3.1 collective-permute-start
  11.2 49.3 %collective-permute-done = bf16[1280,512]{1,0:T(8,128)(2,1)S(1)} collective-permute-done((bf16[1280,512]{1,0:T(8,128)(2,1)}, bf16[1280,512]{1,0:T(8,128)(2,1)S(1)}, u32[]{:S(2)}, u32[]{:S(2)}) %collective-permute-start) | collective-permute-done | bytes 1310752 | tf_op jit(solution)/shard_map/ppermute | solution.py:69
  60.5 21.1 %collective-permute-start.1 = (bf16[1280,512]{1,0:T(8,128)(2,1)S(1)}, bf16[1280,512]{1,0:T(8,128)(2,1)}, u32[]{:S(2)}, u32[]{:S(2)}) collective-permute-start(bf16[1280,512]{1,0:T(8,128)(2,1)S(1)} %collective-permute-done), channel_id=1, source_target_pairs={{0,4},{4,8},{8,12},{12,0},{1,5},{5,9},{9,13},{13,1},{2,6},{6,10},{... | collective-permute-start | bytes 3932168 | tf_op jit(solution)/shard_map/ppermute | solution.py:69
  81.6 57.3 %collective-permute-done.1 = bf16[1280,512]{1,0:T(8,128)(2,1)} collective-permute-done((bf16[1280,512]{1,0:T(8,128)(2,1)S(1)}, bf16[1280,512]{1,0:T(8,128)(2,1)}, u32[]{:S(2)}, u32[]{:S(2)}) %collective-permute-start.1) | collective-permute-done | bytes 1310752 | tf_op jit(solution)/shard_map/ppermute | solution.py:69
  138.9 14.5 %collective-permute-start.2 = (bf16[1280,512]{1,0:T(8,128)(2,1)}, bf16[1280,512]{1,0:T(8,128)(2,1)}, u32[]{:S(2)}, u32[]{:S(2)}) collective-permute-start(bf16[1280,512]{1,0:T(8,128)(2,1)} %collective-permute-done.1), channel_id=1, source_target_pairs={{0,4},{4,8},{8,12},{12,0},{1,5},{5,9},{9,13},{13,1},{2,6},{6,10},{... | collective-permute-start | bytes 3932168 | tf_op jit(solution)/shard_map/ppermute | solution.py:69
  153.3 0.0 copy-done
  153.3 0.4 fusion.4
  153.7 48.9 %collective-permute-done.2 = bf16[1280,512]{1,0:T(8,128)(2,1)} collective-permute-done((bf16[1280,512]{1,0:T(8,128)(2,1)}, bf16[1280,512]{1,0:T(8,128)(2,1)}, u32[]{:S(2)}, u32[]{:S(2)}) %collective-permute-start.2) | collective-permute-done | bytes 1310752 | tf_op jit(solution)/shard_map/ppermute | solution.py:69
  202.7 2.6 constant_dynamic-update-slice_fusion.7
  205.3 2.7 constant_dynamic-update-slice_fusion.6
  207.9 1.3 constant_dynamic-update-slice_fusion.5
  209.2 1.3 constant_dynamic-update-slice_fusion.4
  210.5 2.6 constant_dynamic-update-slice_fusion.3
  213.1 2.6 constant_dynamic-update-slice_fusion.2
  215.6 1.2 constant_dynamic-update-slice_fusion.1
  216.8 1.2 constant_dynamic-update-slice_fusion
  218.1 0.0 copy-done.9
  218.1 6.0 %fusion.68 = f32[384,1280]{1,0:T(8,128)} fusion(bf16[2048,1280]{1,0:T(8,128)(2,1)} %all-gather.4.cloned.1.call-done, bf16[384,2048]{1,0:T(8,128)(2,1)S(1)} %copy-done, f32[2048]{0:T(1024)S(1)} %copy-done.9, f32[384]{0:T(512)S(1)} %add_rsqrt_fusion.2), kind=kOutput, calls=%fused_computation.75 | convolution fusion | flops 2016411648 | bytes 8791552 | tf_op jit(solution)/shard_map/dot_general | solution.py:18
  224.1 45.3 %all-gather.6.cloned.1.call-done = bf16[2048,1280]{1,0:T(8,128)(2,1)} async-done(((bf16[512,1280]{1,0:T(8,128)(2,1)}), bf16[2048,1280]{1,0:T(8,128)(2,1)}) %all-gather.6.cloned.1.call-update) | async-done | bytes 5242896 | tf_op jit(solution)/shard_map/all_gather | solution.py:64
  269.4 10.6 %fusion.18 = bf16[384,2048]{1,0:T(8,128)(2,1)} fusion(bf16[1280,4096]{1,0:T(8,128)(2,1)} %constant_dynamic-update-slice_fusion, s32[]{:T(128)S(6)} %select_n.14, bf16[2048,1280]{1,0:T(8,128)(2,1)} %all-gather.6.cloned.1.call-done, f32[384,1280]{1,0:T(8,128)} %fusion.68, bf16[384,2048]{1,0:T(8,128)(2,1)S(1)} %copy-done, f32[2048]{0:T(1024)S(1)} %copy-done.9, ...), kind=kOutput, calls=%fused_computation.30 | convolution fusion | flops 4033413120 | bytes 15607300 | tf_op jit(solution)/shard_map/dot_general | solution.py:79
  280.1 0.0 all-reduce.4.cloned.1.call-update
  280.1 0.0 all-gather.8.cloned.1.call-start
  280.1 0.0 copy-done.5
  280.2 16.7 %all_gather.14 = bf16[512,4,128]{2,0,1:T(8,128)(2,1)} all-gather(bf16[128,4,128]{2,0,1:T(8,128)(2,1)S(1)} %copy.11), channel_id=1, replica_groups=mesh['grp'=2,'fs'=4,'tp'=4] {'fs'}, dimensions={0}, use_global_device_ids=true | all-gather | bytes 655360 | tf_op jit(solution)/shard_map/all_gather | solution.py:65
  296.9 0.0 all-gather.8.cloned.1.call-update
  296.9 0.2 all-reduce.6.cloned.1.call-start
  297.3 24.9 %all-reduce.4.cloned.1.call-done = bf16[384,2048]{1,0:T(8,128)(2,1)} async-done(((bf16[384,2048]{1,0:T(8,128)(2,1)}), bf16[384,2048]{1,0:T(8,128)(2,1)}) %all-reduce.4.cloned.1.call-update) | async-done | bytes 1572880 | tf_op jit(solution)/shard_map/psum | solution.py:78
  322.1 2.2 fusion.8
  324.4 0.0 copy-done.1
  324.4 3.0 fusion.111
  327.4 19.1 %all-gather.8.cloned.1.call-done = bf16[512,4,512]{2,0,1:T(8,128)(2,1)} async-done(((bf16[512,4,128]{2,0,1:T(8,128)(2,1)}), bf16[512,4,512]{2,0,1:T(8,128)(2,1)}) %all-gather.8.cloned.1.call-update) | async-done | bytes 2097168 | tf_op jit(solution)/shard_map/all_gather | solution.py:73
  346.5 3.0 convolution_add_fusion.3
  349.4 2.9 convolution_add_fusion.2
  352.4 3.0 convolution_add_fusion.1
  355.3 3.0 convolution_add_fusion
  358.3 2.9 fusion.12
  361.2 0.0 copy-start.2
  361.2 1.1 copy-done.2
  362.4 6.0 %fusion.64 = f32[384,1280]{1,0:T(8,128)} fusion(bf16[2048,1280]{1,0:T(8,128)(2,1)} %all-gather.4.cloned.1.call-done, bf16[384,2048]{1,0:T(8,128)(2,1)S(1)} %get-tuple-element.6, f32[2048]{0:T(1024)S(1)} %copy-done.10, f32[384]{0:T(512)S(1)} %add_rsqrt_fusion), kind=kOutput, calls=%fused_computation.74 | convolution fusion | flops 2016411648 | bytes 8791552 | tf_op jit(solution)/shard_map/dot_general | solution.py:18
  368.4 11.2 %fusion.21 = bf16[384,2048]{1,0:T(8,128)(2,1)} fusion(bf16[1280,4096]{1,0:T(8,128)(2,1)} %constant_dynamic-update-slice_fusion, s32[]{:T(128)S(6)} %select_n.14, bf16[2048,1280]{1,0:T(8,128)(2,1)} %all-gather.6.cloned.1.call-done, f32[384,1280]{1,0:T(8,128)} %fusion.64, bf16[384,2048]{1,0:T(8,128)(2,1)} %copy-done.2, f32[2048]{0:T(1024)S(1)} %copy-done.10, ...), kind=kOutput, calls=%fused_computation.31 | convolution fusion | flops 4033413120 | bytes 15607300 | tf_op jit(solution)/shard_map/dot_general | solution.py:90
  379.6 0.0 all-reduce.6.cloned.1.call-update
  379.6 43.0 %all-reduce.6.cloned.1.call-done = bf16[384,2048]{1,0:T(8,128)(2,1)} async-done(((bf16[384,2048]{1,0:T(8,128)(2,1)}), bf16[384,2048]{1,0:T(8,128)(2,1)}) %all-reduce.6.cloned.1.call-update) | async-done | bytes 1572880 | tf_op jit(solution)/shard_map/psum | solution.py:89
  422.6 3.2 fusion.15
  (31 shorter events, 0.1 us)
Async XLA Ops:
  6.5 146.8 %copy-start = (bf16[384,2048]{1,0:T(8,128)(2,1)S(1)}, bf16[384,2048]{1,0:T(8,128)(2,1)}, u32[]{:S(2)}) copy-start(bf16[384,2048]{1,0:T(8,128)(2,1)} %param.10) | copy-start | bytes 4718596
  6.5 211.5 %all-gather.4.cloned.1.call-start = ((), (), s32[]{:S(2)}) async-start(), calls=%async_computation | async-start | bytes 6553600 | tf_op jit(solution)/shard_map/all_gather | solution.py:63
  7.3 262.2 %all-gather.6.cloned.1.call-start = ((), (), s32[]{:S(2)}) async-start(), calls=%async_computation.1 | async-start | bytes 6553600 | tf_op jit(solution)/shard_map/all_gather | solution.py:64
  8.0 314.1 %all-reduce.4.cloned.1.call-start = ((), (), s32[]{:S(2)}) async-start(), calls=%async_computation.2 | async-start | bytes 3145728 | tf_op jit(solution)/shard_map/psum | solution.py:78
  8.1 52.4 %collective-permute-start = (bf16[1280,512]{1,0:T(8,128)(2,1)}, bf16[1280,512]{1,0:T(8,128)(2,1)S(1)}, u32[]{:S(2)}, u32[]{:S(2)}) collective-permute-start(bf16[1280,512]{1,0:T(8,128)(2,1)} %param.13), channel_id=1, source_target_pairs={{0,4},{4,8},{8,12},{12,0},{1,5},{5,9},{9,13},{13,1},{2,6},{6,10},{... | collective-permute-start | bytes 3932168 | tf_op jit(solution)/shard_map/ppermute | solution.py:69
  60.5 78.4 %collective-permute-start.1 = (bf16[1280,512]{1,0:T(8,128)(2,1)S(1)}, bf16[1280,512]{1,0:T(8,128)(2,1)}, u32[]{:S(2)}, u32[]{:S(2)}) collective-permute-start(bf16[1280,512]{1,0:T(8,128)(2,1)S(1)} %collective-permute-done), channel_id=1, source_target_pairs={{0,4},{4,8},{8,12},{12,0},{1,5},{5,9},{9,13},{13,1},{2,6},{6,10},{... | collective-permute-start | bytes 3932168 | tf_op jit(solution)/shard_map/ppermute | solution.py:69
  138.9 63.8 %collective-permute-start.2 = (bf16[1280,512]{1,0:T(8,128)(2,1)}, bf16[1280,512]{1,0:T(8,128)(2,1)}, u32[]{:S(2)}, u32[]{:S(2)}) collective-permute-start(bf16[1280,512]{1,0:T(8,128)(2,1)} %collective-permute-done.1), channel_id=1, source_target_pairs={{0,4},{4,8},{8,12},{12,0},{1,5},{5,9},{9,13},{13,1},{2,6},{6,10},{... | collective-permute-start | bytes 3932168 | tf_op jit(solution)/shard_map/ppermute | solution.py:69
  205.3 4.0 copy-start.4
  215.6 2.5 copy-start.9
  224.1 56.0 %copy-start.5 = (bf16[128,4,128]{2,1,0:T(4,128)(2,1)S(1)}, bf16[128,4,128]{2,1,0:T(4,128)(2,1)}, u32[]{:S(2)}) copy-start(bf16[128,4,128]{2,1,0:T(4,128)(2,1)} %param.14) | copy-start | bytes 393220
  224.1 73.1 %copy-start.8 = (f32[4,512]{1,0:T(4,128)S(1)}, f32[4,512]{1,0:T(4,128)}, u32[]{:S(2)}) copy-start(f32[4,512]{1,0:T(4,128)} %param.15) | copy-start | bytes 24580
  280.1 44.3 %copy-start.6 = (f32[2048]{0:T(1024)S(1)}, f32[2048]{0:T(1024)}, u32[]{:S(2)}) copy-start(f32[2048]{0:T(1024)} %param.18) | copy-start | bytes 24580
  280.1 66.4 %all-gather.8.cloned.1.call-start = ((), (), s32[]{:S(2)}) async-start(), calls=%async_computation.3 | async-start | bytes 2621440 | tf_op jit(solution)/shard_map/all_gather | solution.py:73
  296.9 125.7 %all-reduce.6.cloned.1.call-start = ((), (), s32[]{:S(2)}) async-start(), calls=%async_computation.4 | async-start | bytes 3145728 | tf_op jit(solution)/shard_map/psum | solution.py:89
  322.1 2.2 copy-start.1
  355.3 3.0 copy-start.7
  358.3 4.1 copy-start.10
  361.2 1.1 copy-start.2
  368.4 54.3 %copy-start.3 = (bf16[384,2048]{1,0:T(8,128)(2,1)S(1)}, bf16[384,2048]{1,0:T(8,128)(2,1)}, u32[]{:S(2)}) copy-start(bf16[384,2048]{1,0:T(8,128)(2,1)} %copy-done.2) | copy-start | bytes 4718596
Sparse Core Ops, SparseCore 0:
  8.9 146.1 all-gather.3
  156.7 112.7 all-gather.5
  280.2 41.8 all-reduce.3
  323.5 22.8 all-gather.7
  379.8 42.8 all-reduce.5
